TPU v7x, 512 devices: a whole 4x8x8 slice. The times are simulated.
512 devices in a mesh: sp: 32 (over z, x), tp: 16 (over y, core).
Axes of the slice: x: 4, y: 8, z: 8, core: 2. Of those that a mesh axis runs over, the one named last changes fastest.
Arguments:
- queries: bfloat16 [8192, 1024], P('sp', 'tp'), may hold values from -64 to 64
- keys: bfloat16 [8192, 1024], P('sp', 'tp'), may hold values from -64 to 64
- values: bfloat16 [8192, 1024], P('sp', 'tp'), may hold values from -6 to 6
- cum_gate: float32 [16, 8192], P('tp'), may hold values from -8192 to 0, as said below
- out_weight: bfloat16 [1024, 2048], P('tp'), may hold values from -0.375 to 0.375
- resid: bfloat16 [8192, 2048], P('sp'), may hold values from -6 to 6
- norm_gain: float32 [2048], replicated, may hold values from 0.1 to 1.9
- routes: int32 [8192, 2], P('sp'), may hold values from 0 to 31, all different within a row; in each aligned block of 256 rows (0 to 255, 256 to 511, ...) at most 20 rows name the same one
- route_weight: float32 [8192, 2], P('sp'), may hold values from 0.1 to 0.9
- gate_weight: bfloat16 [32, 2048, 4096], P('sp', None, 'tp'), may hold values from -0.125 to 0.125
- up_weight: bfloat16 [32, 2048, 4096], P('sp', None, 'tp'), may hold values from -0.125 to 0.125
- down_weight: bfloat16 [32, 4096, 2048], P('sp', 'tp'), may hold values from -0.09375 to 0.09375
Outputs:
- layer_out: bfloat16 [8192, 2048], P('sp', 'tp')
Inputs may be any that keep to these rules, and one draw needn't show every extreme that they name: `routes`: each token names 2 different experts. Among the rows of one index of sp, no expert is named more than 20 times, a bound that some block reaches. `cum_gate`: each head's row does not rise along the positions.
All inputs are finite; a program needn't handle non-finite values.
Results may differ from a plain program's by a relative error of at most 0.015.
Values may be sent and summed in bfloat16 or wider, within the bound.
No kernel may reach another device: no remote copies, remote signals or barrier semaphores. Data moves between devices by JAX's collectives and lax.ppermute only.
A program may use at most 64 MiB of HBM per device.

v0:
```python
import math
import jax
import jax.numpy as jnp
from jax import lax
from jax.sharding import PartitionSpec as P

HD = 64
epsilon = 1e-06


def in_one_piece(arrays, axis, dim, along):
    ends, at = ([], 0)
    for a in arrays[:-1]:
        at += a.shape[along]
        ends.append(at)
    both = jnp.concatenate(arrays, axis=along)
    return tuple(jnp.split(lax.all_gather(both, axis, axis=dim, tiled=True), ends, axis=along))


def in_blocks(x, dim, length):
    before, after = (x.shape[:dim], x.shape[dim + 1 :])
    return jnp.moveaxis(x.reshape(*before, length, -1, *after), dim, 0)


def sum_at_owner(x, axis, dim):
    tiles = in_blocks(x, dim, lax.axis_size(axis))
    arrived = lax.all_to_all(tiles, axis, split_axis=0, concat_axis=0, tiled=True)
    return arrived.astype(jnp.float32).sum(axis=0)


def from_everyone(x, axis):
    length = lax.axis_size(axis)
    return lax.all_to_all(jnp.broadcast_to(x[None], (length, *x.shape)), axis, 0, 0, tiled=True)


def of_everyone(x, axis):
    everything = from_everyone(x, axis)
    return jnp.sum(everything, axis=0)


def attend_block(
    carried, query_heads, cum_query, key_rows, value_rows, cum_keys, query_first, key_first
):
    best_score, weight_sum, value_sum = carried
    score_scale = query_heads.shape[-1] ** (-0.5)
    scores = (
        jnp.einsum("hqd,hkd->hqk", query_heads, key_rows, preferred_element_type=jnp.float32)
        * score_scale
    )
    scores = scores + cum_query[:, :, None] - cum_keys[:, None, :]
    query_pos = query_first + jnp.arange(query_heads.shape[1], dtype=jnp.int32)
    key_pos = key_first + jnp.arange(key_rows.shape[1], dtype=jnp.int32)
    permitted_mask = (key_pos[None, :] <= query_pos[:, None])[None]
    new_best = jnp.maximum(
        best_score, jnp.max(jnp.where(permitted_mask, scores, -jnp.inf), axis=-1)
    )
    weights = jnp.where(permitted_mask, jnp.exp(scores - new_best[..., None]), 0.0)
    shrink = jnp.exp(best_score - new_best)
    weight_sum = weight_sum * shrink + jnp.sum(weights, axis=-1)
    value_sum = value_sum * shrink[..., None] + jnp.einsum(
        "hqk,hkd->hqd", weights.astype(jnp.bfloat16), value_rows, preferred_element_type=jnp.float32
    )
    return (new_best, weight_sum, value_sum)


def local(
    queries,
    keys,
    values,
    cum_gate,
    out_weight,
    resid,
    norm_gain,
    routes,
    route_weight,
    gate_weight,
    up_weight,
    down_weight,
):
    rows_here = queries.shape[0]
    heads_here = queries.shape[1] // HD
    sp_count = lax.axis_size("sp")
    tp_count = lax.axis_size("tp")
    shift_amount = lax.axis_index("sp") * rows_here
    model_width = resid.shape[1]
    columns = model_width // tp_count
    column_first = lax.axis_index("tp") * columns
    query_heads = queries.reshape(rows_here, heads_here, HD).transpose(1, 0, 2)
    cum_query = lax.dynamic_slice_in_dim(cum_gate, shift_amount, rows_here, 1)
    start_state = (
        jnp.full((heads_here, rows_here), -1e30, jnp.float32),
        jnp.zeros((heads_here, rows_here), jnp.float32),
        jnp.zeros((heads_here, rows_here, HD), jnp.float32),
    )
    key_part, value_part = in_one_piece((keys, values), "sp", 0, 1)
    piece_rows = key_part.shape[0]
    key_block = math.gcd(piece_rows, 1024)

    def attend_piece(running):

        def key_step(block_index, inner_state):
            block_first = block_index * key_block
            key_rows = lax.dynamic_slice_in_dim(key_part, block_first, key_block, 0)
            key_rows = key_rows.reshape(key_block, heads_here, HD).transpose(1, 0, 2)
            value_rows = lax.dynamic_slice_in_dim(value_part, block_first, key_block, 0)
            value_rows = value_rows.reshape(key_block, heads_here, HD).transpose(1, 0, 2)
            cum_keys = lax.dynamic_slice_in_dim(cum_gate, block_first, key_block, 1)
            return attend_block(
                inner_state,
                query_heads,
                cum_query,
                key_rows,
                value_rows,
                cum_keys,
                shift_amount,
                block_first,
            )

        return lax.fori_loop(0, piece_rows // key_block, key_step, running)

    best_score, weight_sum, value_sum = lax.cond(
        jnp.int32(0) <= shift_amount + rows_here - 1,
        attend_piece,
        lambda running: running,
        start_state,
    )
    attended = (value_sum / weight_sum[..., None]).astype(jnp.bfloat16)
    attended = attended.transpose(1, 0, 2).reshape(rows_here, heads_here * HD)
    partial_value = jnp.dot(attended, out_weight, preferred_element_type=jnp.float32)
    mixed_sum = sum_at_owner(partial_value.astype(jnp.bfloat16), "tp", 1)
    stream_cols = (
        lax.dynamic_slice_in_dim(resid, column_first, columns, 1).astype(jnp.float32) + mixed_sum
    )
    square_sum = of_everyone(jnp.sum(stream_cols * stream_cols, axis=1, keepdims=True), "tp")
    gain_cols = lax.dynamic_slice_in_dim(norm_gain, column_first, columns, 0)
    normed = (stream_cols * lax.rsqrt(square_sum / model_width + epsilon) * gain_cols).astype(
        jnp.bfloat16
    )
    capacity = 5 * rows_here // (2 * sp_count)
    chosen = routes.reshape(-1)
    onehot = (chosen[:, None] == jnp.arange(sp_count, dtype=jnp.int32)[None, :]).astype(jnp.int32)
    before = jnp.cumsum(onehot, axis=0) - onehot
    rank_within = jnp.sum(before * onehot, axis=1)
    slot_index = chosen * capacity + rank_within
    source_row = (
        jnp.zeros((sp_count * capacity,), jnp.int32)
        .at[slot_index]
        .set(jnp.arange(chosen.shape[0], dtype=jnp.int32) // routes.shape[1])
    )
    filled = jnp.zeros((sp_count * capacity,), jnp.bool_).at[slot_index].set(True)
    outgoing = jnp.where(filled[:, None], normed[source_row], jnp.zeros((), jnp.bfloat16))
    outgoing = outgoing.reshape(sp_count, capacity, normed.shape[1])
    gate_here = gate_weight[0]
    up_here = up_weight[0]
    local_down_weight = down_weight[0]
    arrived = lax.all_to_all(outgoing, "sp", split_axis=0, concat_axis=0, tiled=True)
    arrived_rows = arrived.reshape(-1, columns)
    col_part = lax.all_gather(arrived_rows, "tp", axis=1, tiled=True)
    gate_sum = jnp.dot(col_part, gate_here, preferred_element_type=jnp.float32)
    up_sum = jnp.dot(col_part, up_here, preferred_element_type=jnp.float32)
    slot_shape = arrived.shape
    hidden = (jax.nn.silu(gate_sum) * up_sum).astype(jnp.bfloat16)
    partial_term = jnp.dot(hidden, local_down_weight, preferred_element_type=jnp.float32)
    expert_rows = sum_at_owner(partial_term.astype(jnp.bfloat16), "tp", 1).astype(jnp.bfloat16)
    returned = expert_rows.reshape(slot_shape[0], slot_shape[1], columns)
    returned_back = lax.all_to_all(returned, "sp", split_axis=0, concat_axis=0, tiled=True)
    returned_flat = returned_back.reshape(sp_count * capacity, columns)
    picked = (
        returned_flat[slot_index].reshape(rows_here, routes.shape[1], columns).astype(jnp.float32)
    )
    combined = jnp.sum(picked * route_weight[..., None], axis=1)
    return (stream_cols + combined).astype(jnp.bfloat16)


def solution(mesh):
    return jax.shard_map(
        local,
        mesh=mesh,
        in_specs=(
            P("sp", "tp"),
            P("sp", "tp"),
            P("sp", "tp"),
            P("tp", None),
            P("tp", None),
            P("sp", None),
            P(),
            P("sp", None),
            P("sp", None),
            P("sp", None, "tp"),
            P("sp", None, "tp"),
            P("sp", "tp", None),
        ),
        out_specs=P("sp", "tp"),
        check_vma=False,
    )
```

profile of v0, /device:TPU:1, one launch (start us, length us, event | category | flops | bytes accessed | tf_op | source)
XLA Modules:
  0.0 370.9 jit_solution(9054272636798588638)
XLA Ops:
  6.5 1.0 copy.27
  7.5 0.9 copy.28
  8.4 0.7 pad_maximum_fusion
  9.1 86.0 %all-gather.3.cloned.1.call-done = bf16[8192,128]{1,0:T(8,128)(2,1)} async-done(((bf16[256,128]{1,0:T(8,128)(2,1)}), bf16[8192,128]{1,0:T(8,128)(2,1)}) %all-gather.3.cloned.1.call-update) | async-done | bytes 2097168 | tf_op jit(solution)/shard_map/all_gather | solution.py:17
  95.1 49.2 %conditional.1 = (f32[1,256]{1,0:T(1,128)}, f32[1,256,64]{1,2,0:T(8,128)}) conditional(s32[]{:T(128)} %convert_element_type.51, () %tuple.31, (bf16[8192,128]{1,0:T(8,128)(2,1)}, bf16[256,64]{0,1:T(8,128)(2,1)}, s32[]{:T(128)}, f32[1,8192]{1,0:T(1,128)}) %tuple.32), branch_computations={%region_0.0_spmd, %region_1.6_spmd} | conditional | flops 70830592 | bytes 8277405 | solution.py:121
  95.1 0.8 constant_dynamic-slice_fusion.1
  95.9 5.0 %fusion.45 = (bf16[8192,64]{1,0:T(8,128)(2,1)}, bf16[8192,64]{1,0:T(8,128)(2,1)}) fusion(bf16[8192,128]{1,0:T(8,128)(2,1)} %get-tuple-element.217), kind=kLoop, calls=%fused_computation.87 | loop fusion | bytes 4194304 | tf_op jit(solution)/shard_map/split | solution.py:17
  101.0 43.3 %while.20 = (s32[]{:T(128)}, f32[1,256]{1,0:T(1,128)S(1)}, f32[1,256]{1,0:T(1,128)}, f32[1,256,64]{1,2,0:T(8,128)}, s32[]{:T(128)}, /*index=5*/bf16[8192,64]{1,0...) while((s32[]{:T(128)}, f32[1,256]{1,0:T(1,128)S(1)}, ...), condition=%wide.region_5.5_spmd.clone, body=%wide.region_2.4_spmd.clone.sunk | while | flops 70830592 | bytes 3884243 | solution.py:119
  101.0 0.7 constant_dynamic-slice_fusion.3
  101.7 1.4 fusion.58
  103.9 2.0 fusion.62
  105.9 0.7 constant_dynamic-slice_fusion.3
  106.6 1.4 fusion.58
  108.2 1.1 fusion.61
  109.3 2.0 fusion.62
  111.4 0.7 constant_dynamic-slice_fusion.3
  112.1 1.4 fusion.58
  113.7 1.1 fusion.61
  114.8 2.0 fusion.62
  116.9 0.7 constant_dynamic-slice_fusion.3
  117.6 1.4 fusion.58
  119.2 1.1 fusion.61
  120.3 2.0 fusion.62
  122.3 0.7 constant_dynamic-slice_fusion.3
  123.0 1.4 fusion.58
  124.6 1.1 fusion.61
  125.8 2.0 fusion.62
  127.8 0.7 constant_dynamic-slice_fusion.3
  128.5 1.4 fusion.58
  130.1 1.1 fusion.61
  131.3 2.0 fusion.62
  134.0 1.4 fusion.58
  135.6 1.1 fusion.61
  136.8 2.0 fusion.62
  138.8 0.7 constant_dynamic-slice_fusion.3
  139.5 1.4 fusion.58
  141.1 1.1 fusion.61
  142.2 2.0 fusion.62
  144.3 1.3 fusion.22
  145.6 1.3 copy.44
  146.8 12.3 %all-to-all-start = ((bf16[16,256,128]{2,1,0:T(8,128)(2,1)}), bf16[16,256,128]{2,1,0:T(8,128)(2,1)S(1)}, u32[]{:S(2)}, u32[]{:S(2)}) async-start(bf16[16,256,128]{2,1,0:T(8,128)(2,1)} %bitcast.74), calls=%async_computation | async-start | bytes 2097152 | tf_op jit(solution)/shard_map/all_to_all | solution.py:27
  159.6 1.2 reduce-window.6
  161.5 2.4 scatter_custom_fusion.1
  164.0 23.2 %all-to-all-done = bf16[16,256,128]{2,1,0:T(8,128)(2,1)S(1)} async-done(((bf16[16,256,128]{2,1,0:T(8,128)(2,1)}), bf16[16,256,128]{2,1,0:T(8,128)(2,1)S(1)}, u32[]{:S(2)}, u32[]{:S(2)}) %all-to-all-start) | async-done | bytes 1048608 | tf_op jit(solution)/shard_map/all_to_all | solution.py:27
  187.3 1.0 multiply_reduce_fusion
  188.9 3.4 all-to-all-start.1
  192.4 0.8 dynamic_slice.35
  193.2 2.4 scatter_custom_fusion
  195.7 3.9 %all-to-all-done.1 = f32[16,256,1]{1,2,0:T(1,128)S(1)} async-done(((f32[16,256,1]{1,2,0:T(1,128)}), f32[16,256,1]{1,2,0:T(1,128)S(1)}, u32[]{:S(2)}, u32[]{:S(2)}) %all-to-all-start.1) | async-done | bytes 16416 | tf_op jit(solution)/shard_map/all_to_all | solution.py:33
  199.7 0.9 multiply_convert_fusion
  200.7 2.0 gather_fusion
  202.9 15.5 %all_to_all.25 = bf16[32,20,128]{2,1,0:T(8,128)(2,1)S(1)} all-to-all(bf16[32,20,128]{2,1,0:T(8,128)(2,1)S(1)} %broadcast_select_fusion.2), channel_id=1, replica_groups=mesh['sp'=32,'tp'=16] {'sp'}, dimensions={0} | all-to-all | bytes 327680 | tf_op jit(solution)/shard_map/all_to_all | solution.py:156
  218.4 0.7 reshape.154
  219.1 38.1 %all-gather.5.cloned.1.call-done = bf16[640,2048]{1,0:T(8,128)(2,1)} async-done(((bf16[640,128]{1,0:T(8,128)(2,1)}), bf16[640,2048]{1,0:T(8,128)(2,1)}) %all-gather.5.cloned.1.call-update) | async-done | bytes 2621456 | tf_op jit(solution)/shard_map/all_gather | solution.py:158
  257.2 3.4 fusion.26
  260.7 6.2 %fusion.21 = bf16[80,16,8,128]{3,2,1,0:T(8,128)(2,1)} fusion(bf16[1,256,2048]{2,1,0:T(8,128)(2,1)S(1)} %copy-done, bf16[640,2048]{1,0:T(8,128)(2,1)} %all-gather.5.cloned.1.call-done, bf16[1,2048,256]{2,1,0:T(8,128)(2,1)S(1)} %copy-done.6, f32[640,256]{1,0:T(8,128)} %fusion.26), kind=kOutput, calls=%fused_computation.40 | convolution fusion | flops 1344471040 | bytes 7995392 | tf_op jit(solution)/shard_map/dot_general | solution.py:163
  266.9 2.4 copy.43
  269.3 67.0 %all_to_all.26 = bf16[16,640,128]{2,1,0:T(8,128)(2,1)} all-to-all(bf16[16,640,128]{2,1,0:T(8,128)(2,1)S(1)} %bitcast.91), channel_id=1, replica_groups=mesh['sp'=32,'tp'=16] {'tp'}, dimensions={0} | all-to-all | bytes 5242880 | tf_op jit(solution)/shard_map/all_to_all | solution.py:27
  336.3 2.1 reduce_sum.77
  338.5 0.7 reshape.156
  339.2 9.9 %all-to-all-start.4 = ((bf16[32,20,128]{2,1,0:T(8,128)(2,1)}), bf16[32,20,128]{2,1,0:T(8,128)(2,1)S(1)}, u32[]{:S(2)}, u32[]{:S(2)}) async-start(bf16[32,20,128]{2,1,0:T(8,128)(2,1)} %reshape.156), calls=%async_computation.4 | async-start | bytes 393216 | tf_op jit(solution)/shard_map/all_to_all | solution.py:166
  349.3 11.5 %all-to-all-done.4 = bf16[32,20,128]{2,1,0:T(8,128)(2,1)S(1)} async-done(((bf16[32,20,128]{2,1,0:T(8,128)(2,1)}), bf16[32,20,128]{2,1,0:T(8,128)(2,1)S(1)}, u32[]{:S(2)}, u32[]{:S(2)}) %all-to-all-start.4) | async-done | bytes 163872 | tf_op jit(solution)/shard_map/all_to_all | solution.py:166
  360.8 1.3 gather_fusion.1
  362.5 1.5 add_convert_fusion
  (91 shorter events, 6.3 us)
Async XLA Ops:
  6.5 254.1 %copy-start = (bf16[1,256,2048]{2,1,0:T(8,128)(2,1)S(1)}, bf16[1,256,2048]{2,1,0:T(8,128)(2,1)}, u32[]{:S(2)}) copy-start(bf16[1,256,2048]{2,1,0:T(8,128)(2,1)} %param.27) | copy-start | bytes 3145732
  6.5 88.6 %all-gather.3.cloned.1.call-start = ((), (), s32[]{:S(2)}) async-start(), calls=%async_computation.5 | async-start | bytes 2162688 | tf_op jit(solution)/shard_map/all_gather | solution.py:17
  95.1 49.2 %copy-start.1 = (bf16[64,2048]{1,0:T(8,128)(2,1)S(1)}, bf16[64,2048]{1,0:T(8,128)(2,1)}, u32[]{:S(2)}) copy-start(bf16[64,2048]{1,0:T(8,128)(2,1)} %param.20) | copy-start | bytes 786436
  95.9 5.0 %copy-start.2 = (bf16[256,64]{0,1:T(8,128)(2,1)S(1)}, bf16[256,64]{0,1:T(8,128)(2,1)}, u32[]{:S(2)}) copy-start(bf16[256,64]{0,1:T(8,128)(2,1)} %get-tuple-element.272) | copy-start | bytes 98308 | tf_op jit(solution)/shard_map/cond
  144.3 14.9 %copy-start.3 = (s32[256,2]{0,1:T(2,128)S(1)}, s32[256,2]{0,1:T(2,128)}, u32[]{:S(2)}) copy-start(s32[256,2]{0,1:T(2,128)} %param.23) | copy-start | bytes 6148
  146.8 40.3 %all-to-all-start = ((bf16[16,256,128]{2,1,0:T(8,128)(2,1)}), bf16[16,256,128]{2,1,0:T(8,128)(2,1)S(1)}, u32[]{:S(2)}, u32[]{:S(2)}) async-start(bf16[16,256,128]{2,1,0:T(8,128)(2,1)} %bitcast.74), calls=%async_computation | async-start | bytes 2097152 | tf_op jit(solution)/shard_map/all_to_all | solution.py:27
  161.1 96.1 %copy-start.5 = (bf16[1,2048,256]{2,1,0:T(8,128)(2,1)S(1)}, bf16[1,2048,256]{2,1,0:T(8,128)(2,1)}, u32[]{:S(2)}) copy-start(bf16[1,2048,256]{2,1,0:T(8,128)(2,1)} %param.25) | copy-start | bytes 3145732
  188.9 10.8 %all-to-all-start.1 = ((f32[16,256,1]{1,2,0:T(1,128)}), f32[16,256,1]{1,2,0:T(1,128)S(1)}, u32[]{:S(2)}, u32[]{:S(2)}) async-start(f32[16,256,1]{1,2,0:T(1,128)} %broadcast_in_dim.90), calls=%async_computation.1 | async-start | bytes 32768 | tf_op jit(solution)/shard_map/all_to_all | solution.py:33
  192.3 64.9 %all-gather.5.cloned.1.call-start = ((), (), s32[]{:S(2)}) async-start(), calls=%async_computation.6 | async-start | bytes 2785280 | tf_op jit(solution)/shard_map/all_gather | solution.py:158
  219.1 41.5 %copy-start.6 = (bf16[1,2048,256]{2,1,0:T(8,128)(2,1)S(1)}, bf16[1,2048,256]{2,1,0:T(8,128)(2,1)}, u32[]{:S(2)}) copy-start(bf16[1,2048,256]{2,1,0:T(8,128)(2,1)} %param.26) | copy-start | bytes 3145732
  336.3 12.8 %copy-start.4 = (f32[256,2]{0,1:T(2,128)S(1)}, f32[256,2]{0,1:T(2,128)}, u32[]{:S(2)}) copy-start(f32[256,2]{0,1:T(2,128)} %param.24) | copy-start | bytes 6148
  339.2 21.5 %all-to-all-start.4 = ((bf16[32,20,128]{2,1,0:T(8,128)(2,1)}), bf16[32,20,128]{2,1,0:T(8,128)(2,1)S(1)}, u32[]{:S(2)}, u32[]{:S(2)}) async-start(bf16[32,20,128]{2,1,0:T(8,128)(2,1)} %reshape.156), calls=%async_computation.4 | async-start | bytes 393216 | tf_op jit(solution)/shard_map/all_to_all | solution.py:166
Sparse Core Ops, SparseCore 0:
  10.5 84.5 all-gather.2
  219.2 37.9 all-gather.4
where the time goes:
time: 372 us; the launch traced here: 371 us
  waiting for transfers between devices  163 us (44%)
  blocking collectives  82.6 us (22%)
  matrix products  38 us (10%)
  local copies, waits for them, and re-layouts  29.2 us (8%)
  starting transfers between devices  25.7 us (7%)
  other arithmetic  19 us (5%)
  between operations  13.6 us (4%)
    all_gather x1, waiting for transfers between devices, in_one_piece(): lax.all_gather(both, axis, axis=dim, tiled=True)  86 us
    all_to_all x1, blocking collectives, sum_at_owner(): lax.all_to_all(tiles, axis, split_axis=0, concat_axis=0, tiled=True)  67 us
    all_gather x1, waiting for transfers between devices, local(): col_part = lax.all_gather(arrived_rows, 'tp', axis=1, tiled=True)  38.1 us
    all_to_all x1, waiting for transfers between devices, sum_at_owner(): lax.all_to_all(tiles, axis, split_axis=0, concat_axis=0, tiled=True)  23.2 us
    dot_general x8, matrix products, attend_block(): jnp.einsum('hqk,hkd->hqd', weights.astype(jnp.bfloat16), value_rows, pref...  16.2 us
    all_to_all x1, blocking collectives, local(): lax.all_to_all(outgoing, 'sp', split_axis=0, concat_axis=0, tiled=True)  15.5 us
    all_to_all x1, starting transfers between devices, sum_at_owner(): lax.all_to_all(tiles, axis, split_axis=0, concat_axis=0, tiled=True)  12.3 us
    all_to_all x1, waiting for transfers between devices, local(): lax.all_to_all(returned, 'sp', split_axis=0, concat_axis=0, tiled=True)  11.5 us
  transfers between devices with their start and end apart: 5, of which 5 were waited for; matrix products, arithmetic and copies ran while one was open for 2% of the time, Pallas kernels for 0%

commit v1 on v0

--- a/solution.py
+++ b/solution.py
@@ -6,6 +6,12 @@
 
 HD = 64
 epsilon = 1e-06
+
+
+def in_order(tiles, dim):
+    tiles = jnp.moveaxis(tiles, 0, dim)
+    shape = tiles.shape
+    return tiles.reshape(*shape[:dim], shape[dim] * shape[dim + 1], *shape[dim + 2 :])
 
 
 def in_one_piece(arrays, axis, dim, along):
@@ -155,7 +161,19 @@
     local_down_weight = down_weight[0]
     arrived = lax.all_to_all(outgoing, "sp", split_axis=0, concat_axis=0, tiled=True)
     arrived_rows = arrived.reshape(-1, columns)
-    col_part = lax.all_gather(arrived_rows, "tp", axis=1, tiled=True)
+    size = lax.axis_size("tp")
+    pairs = [(i, (i + 1) % size) for i in range(size)]
+    back = [(b, a_2) for a_2, b in pairs]
+    lower, upper = ([], [])
+    for turn in range(size - 1):
+        if turn % 2 == 0:
+            lower.append(lax.ppermute(lower[-1] if lower else arrived_rows, "tp", pairs))
+        else:
+            upper.append(lax.ppermute(upper[-1] if upper else arrived_rows, "tp", back))
+    tiles_2 = jnp.stack([*lower[::-1], arrived_rows, *upper])
+    shift = lax.axis_index("tp") - len(lower)
+    tiles_2 = tiles_2[(jnp.arange(size) - shift) % size]
+    col_part = in_order(tiles_2, 1)
     gate_sum = jnp.dot(col_part, gate_here, preferred_element_type=jnp.float32)
     up_sum = jnp.dot(col_part, up_here, preferred_element_type=jnp.float32)
     slot_shape = arrived.shape

time: 372 us -> 398 us (1.070)
  starting transfers between devices: 25.7 us -> 54.2 us
  waiting for transfers between devices: 163 us -> 135 us
  local copies, waits for them, and re-layouts: 29.2 us -> 49.8 us
    all_gather x1 -> x0, waiting for transfers between devices: 38.1 us -> none  [local(): col_part = lax.all_gather(arrived_rows, 'tp', axis=1, tiled=True)]
    ppermute x0 -> x15, starting transfers between devices: none -> 34.6 us  [the longest x7 25.5 us: local(): upper.append(lax.ppermute(upper[-1] if upper else arrived_rows, 'tp', back))]
    unnamed x16 -> x31, local copies, waits for them, and re-layouts: 2.13 us -> 14.1 us
    ppermute x0 -> x15, waiting for transfers between devices: none -> 10.3 us  [the longest x8 9.13 us: local(): lax.ppermute(lower[-1] if lower else arrived_rows, 'tp', pairs)]
    all_to_all x1, starting transfers between devices: 9.9 us -> 3.86 us  [local(): lax.all_to_all(returned, 'sp', split_axis=0, concat_axis=0, tiled=True)]
    transpose x0 -> x1, local copies, waits for them, and re-layouts: none -> 4.48 us  [in_order(): tiles = jnp.moveaxis(tiles, 0, dim)]
    gather x0 -> x1, local copies, waits for them, and re-layouts: none -> 4.15 us  [local(): tiles_2 = tiles_2[(jnp.arange(size) - shift) % size]]
  transfers between devices with their start and end apart: 5 -> 19, of which waited for: 5 -> 17; matrix products, arithmetic and copies ran while one was open for 2% -> 5% of each run, Pallas kernels for 0% -> 0%
where the time goes in v1:
time: 398 us; the launch traced here: 396 us
  waiting for transfers between devices  135 us (34%)
  blocking collectives  86 us (22%)
  starting transfers between devices  54.2 us (14%)
  local copies, waits for them, and re-layouts  49.8 us (13%)
  matrix products  38.1 us (10%)
  other arithmetic  19.8 us (5%)
  between operations  13.7 us (3%)
    all_gather x1, waiting for transfers between devices, in_one_piece(): lax.all_gather(both, axis, axis=dim, tiled=True)  86 us
    all_to_all x1, blocking collectives, sum_at_owner(): lax.all_to_all(tiles, axis, split_axis=0, concat_axis=0, tiled=True)  70.4 us
    ppermute x7, starting transfers between devices, local(): upper.append(lax.ppermute(upper[-1] if upper else arrived_rows, 'tp', back))  25.5 us
    all_to_all x1, waiting for transfers between devices, sum_at_owner(): lax.all_to_all(tiles, axis, split_axis=0, concat_axis=0, tiled=True)  23.2 us
    dot_general x8, matrix products, attend_block(): jnp.einsum('hqk,hkd->hqd', weights.astype(jnp.bfloat16), value_rows, pref...  16.2 us
    all_to_all x1, blocking collectives, local(): lax.all_to_all(outgoing, 'sp', split_axis=0, concat_axis=0, tiled=True)  15.5 us
    unnamed x31, local copies, waits for them, and re-layouts  14.1 us
    all_to_all x1, starting transfers between devices, sum_at_owner(): lax.all_to_all(tiles, axis, split_axis=0, concat_axis=0, tiled=True)  12.4 us
  transfers between devices with their start and end apart: 19, of which 17 were waited for; matrix products, arithmetic and copies ran while one was open for 5% of the time, Pallas kernels for 0%

profile of v1, /device:TPU:1, one launch (start us, length us, event | category | flops | bytes accessed | tf_op | source)
XLA Modules:
  0.0 396.4 jit_solution(5875811501392070888)
XLA Ops:
  9.1 86.0 %all-gather.2.cloned.1.call-done = bf16[8192,128]{1,0:T(8,128)(2,1)} async-done(((bf16[256,128]{1,0:T(8,128)(2,1)}), bf16[8192,128]{1,0:T(8,128)(2,1)}) %all-gather.2.cloned.1.call-update) | async-done | bytes 2097168 | tf_op jit(solution)/shard_map/all_gather | solution.py:23
  95.1 50.0 %conditional.1 = (f32[1,256]{1,0:T(1,128)}, f32[1,256,64]{1,2,0:T(8,128)}) conditional(s32[]{:T(128)} %convert_element_type.51, () %tuple.31, (bf16[8192,128]{1,0:T(8,128)(2,1)}, bf16[256,64]{0,1:T(8,128)(2,1)}, s32[]{:T(128)}, f32[1,8192]{1,0:T(1,128)}) %tuple.32), branch_computations={%region_0.0_spmd, %region_1.6_spmd} | conditional | flops 70830592 | bytes 8277405 | solution.py:127
  95.9 5.0 %fusion.47 = (bf16[8192,64]{1,0:T(8,128)(2,1)}, bf16[8192,64]{1,0:T(8,128)(2,1)}) fusion(bf16[8192,128]{1,0:T(8,128)(2,1)} %get-tuple-element.217), kind=kLoop, calls=%fused_computation.111 | loop fusion | bytes 4194304 | tf_op jit(solution)/shard_map/split | solution.py:23
  101.0 44.1 %while.20 = (s32[]{:T(128)}, f32[1,256]{1,0:T(1,128)S(1)}, f32[1,256]{1,0:T(1,128)}, f32[1,256,64]{1,2,0:T(8,128)}, s32[]{:T(128)}, /*index=5*/bf16[8192,64]{1,0...) while((s32[]{:T(128)}, f32[1,256]{1,0:T(1,128)S(1)}, ...), condition=%wide.region_5.5_spmd.clone, body=%wide.region_2.4_spmd.clone.sunk | while | flops 70830592 | bytes 3884243 | solution.py:125
  101.7 1.4 fusion.60
  103.9 2.0 fusion.64
  106.7 1.4 fusion.60
  108.3 1.3 fusion.63
  109.5 2.0 fusion.64
  112.3 1.4 fusion.60
  113.9 1.3 fusion.63
  115.1 2.0 fusion.64
  117.8 1.4 fusion.60
  119.5 1.3 fusion.63
  120.7 2.0 fusion.64
  123.4 1.4 fusion.60
  125.0 1.3 fusion.63
  126.3 2.0 fusion.64
  129.0 1.4 fusion.60
  130.6 1.3 fusion.63
  131.9 2.0 fusion.64
  134.6 1.4 fusion.60
  136.2 1.3 fusion.63
  137.5 2.0 fusion.64
  140.2 1.4 fusion.60
  141.8 1.3 fusion.63
  143.1 2.0 fusion.64
  145.1 1.3 fusion.22
  146.4 1.3 copy.46
  147.7 12.4 %all-to-all-start = ((bf16[16,256,128]{2,1,0:T(8,128)(2,1)}), bf16[16,256,128]{2,1,0:T(8,128)(2,1)S(1)}, u32[]{:S(2)}, u32[]{:S(2)}) async-start(bf16[16,256,128]{2,1,0:T(8,128)(2,1)} %bitcast.108), calls=%async_computation | async-start | bytes 2097152 | tf_op jit(solution)/shard_map/all_to_all | solution.py:33
  160.5 1.2 reduce-window.6
  162.4 2.4 scatter_custom_fusion.1
  164.8 23.2 %all-to-all-done = bf16[16,256,128]{2,1,0:T(8,128)(2,1)S(1)} async-done(((bf16[16,256,128]{2,1,0:T(8,128)(2,1)}), bf16[16,256,128]{2,1,0:T(8,128)(2,1)S(1)}, u32[]{:S(2)}, u32[]{:S(2)}) %all-to-all-start) | async-done | bytes 1048608 | tf_op jit(solution)/shard_map/all_to_all | solution.py:33
  189.8 3.4 all-to-all-start.1
  194.0 2.4 scatter_custom_fusion
  196.5 4.0 %all-to-all-done.1 = f32[16,256,1]{1,2,0:T(1,128)S(1)} async-done(((f32[16,256,1]{1,2,0:T(1,128)}), f32[16,256,1]{1,2,0:T(1,128)S(1)}, u32[]{:S(2)}, u32[]{:S(2)}) %all-to-all-start.1) | async-done | bytes 16416 | tf_op jit(solution)/shard_map/all_to_all | solution.py:39
  201.5 2.0 gather_fusion
  203.7 15.5 %all_to_all.25 = bf16[32,20,128]{2,1,0:T(8,128)(2,1)S(1)} all-to-all(bf16[32,20,128]{2,1,0:T(8,128)(2,1)S(1)} %broadcast_select_fusion.2), channel_id=1, replica_groups=mesh['sp'=32,'tp'=16] {'sp'}, dimensions={0} | all-to-all | bytes 327680 | tf_op jit(solution)/shard_map/all_to_all | solution.py:162
  219.3 2.1 collective-permute-start
  221.4 2.3 collective-permute-done
  223.7 2.5 collective-permute-start.1
  227.2 1.2 collective-permute-done.1
  228.4 2.5 collective-permute-start.2
  231.2 2.0 collective-permute-start.9
  234.0 1.6 collective-permute-start.3
  235.9 3.2 collective-permute-start.10
  240.7 4.4 %collective-permute-start.11 = (bf16[640,128]{1,0:T(8,128)(2,1)S(1)}, bf16[640,128]{1,0:T(8,128)(2,1)S(1)}, u32[]{:S(2)}, u32[]{:S(2)}) collective-permute-start(bf16[640,128]{1,0:T(8,128)(2,1)S(1)} %collective-permute-done.10), channel_id=1, source_target_pairs={{1,0},{2,1},{3,2},{4,3},{5,4},{6,5},{7,6},{8,7},{9,8},{10,9},{11,1... | collective-permute-start | bytes 491528 | tf_op jit(solution)/shard_map/ppermute | solution.py:172
  246.1 4.9 %collective-permute-start.12 = (bf16[640,128]{1,0:T(8,128)(2,1)S(1)}, bf16[640,128]{1,0:T(8,128)(2,1)S(1)}, u32[]{:S(2)}, u32[]{:S(2)}) collective-permute-start(bf16[640,128]{1,0:T(8,128)(2,1)S(1)} %collective-permute-done.11), channel_id=1, source_target_pairs={{1,0},{2,1},{3,2},{4,3},{5,4},{6,5},{7,6},{8,7},{9,8},{10,9},{11,1... | collective-permute-start | bytes 491528 | tf_op jit(solution)/shard_map/ppermute | solution.py:172
  252.1 4.9 %collective-permute-start.13 = (bf16[640,128]{1,0:T(8,128)(2,1)S(1)}, bf16[640,128]{1,0:T(8,128)(2,1)S(1)}, u32[]{:S(2)}, u32[]{:S(2)}) collective-permute-start(bf16[640,128]{1,0:T(8,128)(2,1)S(1)} %collective-permute-done.12), channel_id=1, source_target_pairs={{1,0},{2,1},{3,2},{4,3},{5,4},{6,5},{7,6},{8,7},{9,8},{10,9},{11,1... | collective-permute-start | bytes 491528 | tf_op jit(solution)/shard_map/ppermute | solution.py:172
  258.1 5.1 %collective-permute-start.14 = (bf16[640,128]{1,0:T(8,128)(2,1)S(1)}, bf16[640,128]{1,0:T(8,128)(2,1)S(1)}, u32[]{:S(2)}, u32[]{:S(2)}) collective-permute-start(bf16[640,128]{1,0:T(8,128)(2,1)S(1)} %collective-permute-done.13), channel_id=1, source_target_pairs={{1,0},{2,1},{3,2},{4,3},{5,4},{6,5},{7,6},{8,7},{9,8},{10,9},{11,1... | collective-permute-start | bytes 491528 | tf_op jit(solution)/shard_map/ppermute | solution.py:172
  263.1 1.1 collective-permute-done.7
  264.3 1.6 bitcast_dynamic-update-slice_fusion.14
  265.9 1.6 bitcast_dynamic-update-slice_fusion.13
  276.9 4.1 %gather_fusion.1 = bf16[16,640,128]{2,1,0:T(8,128)(2,1)} fusion(bf16[16,640,128]{2,1,0:T(8,128)(2,1)} %bitcast_dynamic-update-slice_fusion, s32[1024]{0:T(1024)S(1)} %pad_clamp_fusion.1), kind=kCustom, calls=%fused_computation.1 | custom fusion | bytes 5242944 | tf_op jit(solution)/shard_map/gather | solution.py:175
  281.1 4.5 %copy.36 = bf16[640,16,128]{0,2,1:T(8,128)(2,1)} copy(bf16[640,16,128]{2,0,1:T(8,128)(2,1)} %bitcast.125) | data formatting | bytes 5242880 | tf_op jit(solution)/shard_map/transpose | solution.py:12
  285.5 3.6 fusion.26
  289.1 6.2 %fusion.21 = bf16[80,16,8,128]{3,2,1,0:T(8,128)(2,1)} fusion(bf16[1,256,2048]{2,1,0:T(8,128)(2,1)S(1)} %copy-done, bf16[640,2048]{0,1:T(8,128)(2,1)} %bitcast.128, bf16[1,2048,256]{2,1,0:T(8,128)(2,1)S(1)} %copy-done.6, f32[640,256]{1,0:T(8,128)} %fusion.26), kind=kOutput, calls=%fused_computation.41 | convolution fusion | flops 1344471040 | bytes 7995392 | tf_op jit(solution)/shard_map/dot_general | solution.py:181
  295.4 2.4 copy.45
  297.8 70.4 %all_to_all.26 = bf16[16,640,128]{2,1,0:T(8,128)(2,1)} all-to-all(bf16[16,640,128]{2,1,0:T(8,128)(2,1)S(1)} %bitcast.126), channel_id=1, replica_groups=mesh['sp'=32,'tp'=16] {'tp'}, dimensions={0} | all-to-all | bytes 5242880 | tf_op jit(solution)/shard_map/all_to_all | solution.py:33
  368.2 2.1 reduce_sum.77
  371.1 3.9 all-to-all-start.4
  375.1 11.1 %all-to-all-done.4 = bf16[32,20,128]{2,1,0:T(8,128)(2,1)S(1)} async-done(((bf16[32,20,128]{2,1,0:T(8,128)(2,1)}), bf16[32,20,128]{2,1,0:T(8,128)(2,1)S(1)}, u32[]{:S(2)}, u32[]{:S(2)}) %all-to-all-start.4) | async-done | bytes 163872 | tf_op jit(solution)/shard_map/all_to_all | solution.py:184
  386.2 1.3 gather_fusion.2
  388.0 1.5 add_convert_fusion
  (139 shorter events, 34.6 us)
Async XLA Ops:
  6.5 282.6 %copy-start = (bf16[1,256,2048]{2,1,0:T(8,128)(2,1)S(1)}, bf16[1,256,2048]{2,1,0:T(8,128)(2,1)}, u32[]{:S(2)}) copy-start(bf16[1,256,2048]{2,1,0:T(8,128)(2,1)} %param.27) | copy-start | bytes 3145732
  6.5 88.6 %all-gather.2.cloned.1.call-start = ((), (), s32[]{:S(2)}) async-start(), calls=%async_computation.5 | async-start | bytes 2162688 | tf_op jit(solution)/shard_map/all_gather | solution.py:23
  95.1 50.0 %copy-start.1 = (bf16[64,2048]{1,0:T(8,128)(2,1)S(1)}, bf16[64,2048]{1,0:T(8,128)(2,1)}, u32[]{:S(2)}) copy-start(bf16[64,2048]{1,0:T(8,128)(2,1)} %param.20) | copy-start | bytes 786436
  95.9 5.0 %copy-start.2 = (bf16[256,64]{0,1:T(8,128)(2,1)S(1)}, bf16[256,64]{0,1:T(8,128)(2,1)}, u32[]{:S(2)}) copy-start(bf16[256,64]{0,1:T(8,128)(2,1)} %get-tuple-element.272) | copy-start | bytes 98308 | tf_op jit(solution)/shard_map/cond
  145.1 14.9 %copy-start.3 = (s32[256,2]{0,1:T(2,128)S(1)}, s32[256,2]{0,1:T(2,128)}, u32[]{:S(2)}) copy-start(s32[256,2]{0,1:T(2,128)} %param.23) | copy-start | bytes 6148
  147.7 40.4 %all-to-all-start = ((bf16[16,256,128]{2,1,0:T(8,128)(2,1)}), bf16[16,256,128]{2,1,0:T(8,128)(2,1)S(1)}, u32[]{:S(2)}, u32[]{:S(2)}) async-start(bf16[16,256,128]{2,1,0:T(8,128)(2,1)} %bitcast.108), calls=%async_computation | async-start | bytes 2097152 | tf_op jit(solution)/shard_map/all_to_all | solution.py:33
  189.8 10.8 %all-to-all-start.1 = ((f32[16,256,1]{1,2,0:T(1,128)}), f32[16,256,1]{1,2,0:T(1,128)S(1)}, u32[]{:S(2)}, u32[]{:S(2)}) async-start(f32[16,256,1]{1,2,0:T(1,128)} %broadcast_in_dim.91), calls=%async_computation.1 | async-start | bytes 32768 | tf_op jit(solution)/shard_map/all_to_all | solution.py:39
  219.3 4.4 %collective-permute-start = (bf16[640,128]{1,0:T(8,128)(2,1)S(1)}, bf16[640,128]{1,0:T(8,128)(2,1)S(1)}, u32[]{:S(2)}, u32[]{:S(2)}) collective-permute-start(bf16[640,128]{1,0:T(8,128)(2,1)S(1)} %reshape.206), channel_id=1, source_target_pairs={{0,1},{1,2},{2,3},{3,4},{4,5},{5,6},{6,7},{7,8},{8,9},{9,10},{10,1... | collective-permute-start | bytes 491528 | tf_op jit(solution)/shard_map/ppermute | solution.py:170
  223.7 4.7 %collective-permute-start.1 = (bf16[640,128]{1,0:T(8,128)(2,1)S(1)}, bf16[640,128]{1,0:T(8,128)(2,1)S(1)}, u32[]{:S(2)}, u32[]{:S(2)}) collective-permute-start(bf16[640,128]{1,0:T(8,128)(2,1)S(1)} %collective-permute-done), channel_id=1, source_target_pairs={{0,1},{1,2},{2,3},{3,4},{4,5},{5,6},{6,7},{7,8},{8,9},{9,10},{10,1... | collective-permute-start | bytes 491528 | tf_op jit(solution)/shard_map/ppermute | solution.py:170
  226.1 5.0 %collective-permute-start.8 = (bf16[640,128]{1,0:T(8,128)(2,1)S(1)}, bf16[640,128]{1,0:T(8,128)(2,1)S(1)}, u32[]{:S(2)}, u32[]{:S(2)}) collective-permute-start(bf16[640,128]{1,0:T(8,128)(2,1)S(1)} %reshape.206), channel_id=1, source_target_pairs={{1,0},{2,1},{3,2},{4,3},{5,4},{6,5},{7,6},{8,7},{9,8},{10,9},{11,1... | collective-permute-start | bytes 491528 | tf_op jit(solution)/shard_map/ppermute | solution.py:172
  228.4 5.6 %collective-permute-start.2 = (bf16[640,128]{1,0:T(8,128)(2,1)S(1)}, bf16[640,128]{1,0:T(8,128)(2,1)S(1)}, u32[]{:S(2)}, u32[]{:S(2)}) collective-permute-start(bf16[640,128]{1,0:T(8,128)(2,1)S(1)} %collective-permute-done.1), channel_id=1, source_target_pairs={{0,1},{1,2},{2,3},{3,4},{4,5},{5,6},{6,7},{7,8},{8,9},{9,10},{10,1... | collective-permute-start | bytes 491528 | tf_op jit(solution)/shard_map/ppermute | solution.py:170
  231.2 4.7 %collective-permute-start.9 = (bf16[640,128]{1,0:T(8,128)(2,1)S(1)}, bf16[640,128]{1,0:T(8,128)(2,1)S(1)}, u32[]{:S(2)}, u32[]{:S(2)}) collective-permute-start(bf16[640,128]{1,0:T(8,128)(2,1)S(1)} %collective-permute-done.8), channel_id=1, source_target_pairs={{1,0},{2,1},{3,2},{4,3},{5,4},{6,5},{7,6},{8,7},{9,8},{10,9},{11,1... | collective-permute-start | bytes 491528 | tf_op jit(solution)/shard_map/ppermute | solution.py:172
  234.0 6.0 %collective-permute-start.3 = (bf16[640,128]{1,0:T(8,128)(2,1)S(1)}, bf16[640,128]{1,0:T(8,128)(2,1)S(1)}, u32[]{:S(2)}, u32[]{:S(2)}) collective-permute-start(bf16[640,128]{1,0:T(8,128)(2,1)S(1)} %collective-permute-done.2), channel_id=1, source_target_pairs={{0,1},{1,2},{2,3},{3,4},{4,5},{5,6},{6,7},{7,8},{8,9},{9,10},{10,1... | collective-permute-start | bytes 491528 | tf_op jit(solution)/shard_map/ppermute | solution.py:170
  235.9 4.7 %collective-permute-start.10 = (bf16[640,128]{1,0:T(8,128)(2,1)S(1)}, bf16[640,128]{1,0:T(8,128)(2,1)S(1)}, u32[]{:S(2)}, u32[]{:S(2)}) collective-permute-start(bf16[640,128]{1,0:T(8,128)(2,1)S(1)} %collective-permute-done.9), channel_id=1, source_target_pairs={{1,0},{2,1},{3,2},{4,3},{5,4},{6,5},{7,6},{8,7},{9,8},{10,9},{11,1... | collective-permute-start | bytes 491528 | tf_op jit(solution)/shard_map/ppermute | solution.py:172
  240.0 6.0 %collective-permute-start.4 = (bf16[640,128]{1,0:T(8,128)(2,1)S(1)}, bf16[640,128]{1,0:T(8,128)(2,1)S(1)}, u32[]{:S(2)}, u32[]{:S(2)}) collective-permute-start(bf16[640,128]{1,0:T(8,128)(2,1)S(1)} %collective-permute-done.3), channel_id=1, source_target_pairs={{0,1},{1,2},{2,3},{3,4},{4,5},{5,6},{6,7},{7,8},{8,9},{9,10},{10,1... | collective-permute-start | bytes 491528 | tf_op jit(solution)/shard_map/ppermute | solution.py:170
  240.7 5.4 %collective-permute-start.11 = (bf16[640,128]{1,0:T(8,128)(2,1)S(1)}, bf16[640,128]{1,0:T(8,128)(2,1)S(1)}, u32[]{:S(2)}, u32[]{:S(2)}) collective-permute-start(bf16[640,128]{1,0:T(8,128)(2,1)S(1)} %collective-permute-done.10), channel_id=1, source_target_pairs={{1,0},{2,1},{3,2},{4,3},{5,4},{6,5},{7,6},{8,7},{9,8},{10,9},{11,1... | collective-permute-start | bytes 491528 | tf_op jit(solution)/shard_map/ppermute | solution.py:172
  246.0 6.0 %collective-permute-start.5 = (bf16[640,128]{1,0:T(8,128)(2,1)S(1)}, bf16[640,128]{1,0:T(8,128)(2,1)S(1)}, u32[]{:S(2)}, u32[]{:S(2)}) collective-permute-start(bf16[640,128]{1,0:T(8,128)(2,1)S(1)} %collective-permute-done.4), channel_id=1, source_target_pairs={{0,1},{1,2},{2,3},{3,4},{4,5},{5,6},{6,7},{7,8},{8,9},{9,10},{10,1... | collective-permute-start | bytes 491528 | tf_op jit(solution)/shard_map/ppermute | solution.py:170
  246.1 6.0 %collective-permute-start.12 = (bf16[640,128]{1,0:T(8,128)(2,1)S(1)}, bf16[640,128]{1,0:T(8,128)(2,1)S(1)}, u32[]{:S(2)}, u32[]{:S(2)}) collective-permute-start(bf16[640,128]{1,0:T(8,128)(2,1)S(1)} %collective-permute-done.11), channel_id=1, source_target_pairs={{1,0},{2,1},{3,2},{4,3},{5,4},{6,5},{7,6},{8,7},{9,8},{10,9},{11,1... | collective-permute-start | bytes 491528 | tf_op jit(solution)/shard_map/ppermute | solution.py:172
  251.9 6.1 %collective-permute-start.6 = (bf16[640,128]{1,0:T(8,128)(2,1)S(1)}, bf16[640,128]{1,0:T(8,128)(2,1)}, u32[]{:S(2)}, u32[]{:S(2)}) collective-permute-start(bf16[640,128]{1,0:T(8,128)(2,1)S(1)} %collective-permute-done.5), channel_id=1, source_target_pairs={{0,1},{1,2},{2,3},{3,4},{4,5},{5,6},{6,7},{7,8},{8,9},{9,10},{10,1... | collective-permute-start | bytes 491528 | tf_op jit(solution)/shard_map/ppermute | solution.py:170
  252.1 6.0 %collective-permute-start.13 = (bf16[640,128]{1,0:T(8,128)(2,1)S(1)}, bf16[640,128]{1,0:T(8,128)(2,1)S(1)}, u32[]{:S(2)}, u32[]{:S(2)}) collective-permute-start(bf16[640,128]{1,0:T(8,128)(2,1)S(1)} %collective-permute-done.12), channel_id=1, source_target_pairs={{1,0},{2,1},{3,2},{4,3},{5,4},{6,5},{7,6},{8,7},{9,8},{10,9},{11,1... | collective-permute-start | bytes 491528 | tf_op jit(solution)/shard_map/ppermute | solution.py:172
  258.0 6.3 %collective-permute-start.7 = (bf16[640,128]{1,0:T(8,128)(2,1)}, bf16[640,128]{1,0:T(8,128)(2,1)}, u32[]{:S(2)}, u32[]{:S(2)}) collective-permute-start(bf16[640,128]{1,0:T(8,128)(2,1)} %collective-permute-done.6), channel_id=1, source_target_pairs={{0,1},{1,2},{2,3},{3,4},{4,5},{5,6},{6,7},{7,8},{8,9},{9,10},{10,1... | collective-permute-start | bytes 491528 | tf_op jit(solution)/shard_map/ppermute | solution.py:170
  258.1 18.1 %collective-permute-start.14 = (bf16[640,128]{1,0:T(8,128)(2,1)S(1)}, bf16[640,128]{1,0:T(8,128)(2,1)S(1)}, u32[]{:S(2)}, u32[]{:S(2)}) collective-permute-start(bf16[640,128]{1,0:T(8,128)(2,1)S(1)} %collective-permute-done.13), channel_id=1, source_target_pairs={{1,0},{2,1},{3,2},{4,3},{5,4},{6,5},{7,6},{8,7},{9,8},{10,9},{11,1... | collective-permute-start | bytes 491528 | tf_op jit(solution)/shard_map/ppermute | solution.py:172
  281.1 4.5 %copy-start.5 = (bf16[1,2048,256]{2,1,0:T(8,128)(2,1)S(1)}, bf16[1,2048,256]{2,1,0:T(8,128)(2,1)}, u32[]{:S(2)}) copy-start(bf16[1,2048,256]{2,1,0:T(8,128)(2,1)} %param.25) | copy-start | bytes 3145732
  285.5 3.6 copy-start.6
  368.2 6.7 %copy-start.4 = (f32[256,2]{0,1:T(2,128)S(1)}, f32[256,2]{0,1:T(2,128)}, u32[]{:S(2)}) copy-start(f32[256,2]{0,1:T(2,128)} %param.24) | copy-start | bytes 6148
  371.1 15.1 %all-to-all-start.4 = ((bf16[32,20,128]{2,1,0:T(8,128)(2,1)}), bf16[32,20,128]{2,1,0:T(8,128)(2,1)S(1)}, u32[]{:S(2)}, u32[]{:S(2)}) async-start(bf16[32,20,128]{2,1,0:T(8,128)(2,1)} %reshape.209), calls=%async_computation.4 | async-start | bytes 393216 | tf_op jit(solution)/shard_map/all_to_all | solution.py:184
Sparse Core Ops, SparseCore 0:
  10.5 84.5 all-gather.1
